TPU v7x, 32 devices: a whole 2x2x4 slice. The times are simulated.
32 devices in a mesh: fs: 8 (over z, x), tp: 4 (over y, core).
Axes of the slice: x: 2, y: 2, z: 4, core: 2. Of those that a mesh axis runs over, the one named last changes fastest.
Arguments:
- tokens: bfloat16 [3584, 2304], P('fs'), may hold values from -6 to 6
- norm_gain: float32 [2304], replicated, may hold values from 0.1 to 1.9
- gate_weight: bfloat16 [2304, 6144], P('fs', 'tp'), may hold values from -0.125 to 0.125
- up_weight: bfloat16 [2304, 6144], P('fs', 'tp'), may hold values from -0.125 to 0.125
- down_weight: bfloat16 [6144, 2304], P('tp', 'fs'), may hold values from -0.078125 to 0.078125
- branch_gain: float32 [2304], replicated, may hold values from 0.1 to 1.9
Outputs:
- result: bfloat16 [3584, 2304], P('fs')
All inputs are finite; a program needn't handle non-finite values.
Results may differ from a plain program's by a relative error of at most 0.014.
Values may be sent and summed in bfloat16 or wider, within the bound.
A program may use at most 64 MiB of HBM per device.

v0:
```python
import jax
import jax.numpy as jnp
from jax import lax
from jax.sharding import PartitionSpec as P

epsilon = 1e-06


def complete(own_tokens, summed, branch_gain):
    branch_scale = lax.rsqrt(jnp.mean(summed * summed, axis=-1, keepdims=True) + epsilon)
    return (own_tokens.astype(jnp.float32) + summed * branch_scale * branch_gain).astype(
        jnp.bfloat16
    )


def per_device(tokens, norm_gain, gate_weight, up_weight, down_weight, branch_gain):
    widened = tokens.astype(jnp.float32)
    scale = lax.rsqrt(jnp.mean(widened * widened, axis=-1, keepdims=True) + epsilon)
    normed = (widened * scale * norm_gain).astype(jnp.bfloat16)
    gate_whole, up_whole = (
        lax.all_gather(gate_weight, "fs", axis=0, tiled=True),
        lax.all_gather(up_weight, "fs", axis=0, tiled=True),
    )
    gate_sum = jnp.dot(normed, gate_whole, preferred_element_type=jnp.float32)
    up_sum = jnp.dot(normed, up_whole, preferred_element_type=jnp.float32)
    hidden = (jax.nn.silu(gate_sum) * up_sum).astype(jnp.bfloat16)
    partial_value = jnp.dot(
        hidden,
        lax.all_gather(down_weight, "fs", axis=1, tiled=True),
        preferred_element_type=jnp.float32,
    )
    summed = lax.psum(partial_value.astype(jnp.bfloat16), "tp").astype(jnp.float32)
    return complete(tokens, summed, branch_gain)


def solution(mesh):
    in_specs = (P("fs", None), P(), P("fs", "tp"), P("fs", "tp"), P("tp", "fs"), P())
    out_specs = P("fs", None)
    return jax.shard_map(
        per_device, mesh=mesh, in_specs=in_specs, out_specs=out_specs, check_vma=False
    )
```

profile of v0, /device:TPU:0, one launch (start us, length us, event | category | flops | bytes accessed | tf_op | source)
XLA Modules:
  0.0 413.5 jit_solution(9930593498482018361)
XLA Ops:
  6.5 0.0 copy-start
  6.5 0.0 copy-start.2
  6.5 0.0 all-gather.4.cloned.1.call-start
  6.5 0.7 all-gather.4.cloned.1.call-update
  7.3 0.0 all-gather.6.cloned.1.call-start
  7.3 0.7 all-gather.6.cloned.1.call-update
  8.0 0.0 all-gather.8.cloned.1.call-start
  8.1 0.7 all-gather.8.cloned.1.call-update
  8.7 0.0 all-reduce.2.cloned.1.call-start
  8.8 2.1 fusion.2
  10.9 109.7 %all-gather.4.cloned.1.call-done = bf16[2304,1536]{1,0:T(8,128)(2,1)} async-done(((bf16[288,1536]{1,0:T(8,128)(2,1)}), bf16[2304,1536]{1,0:T(8,128)(2,1)}) %all-gather.4.cloned.1.call-update) | async-done | bytes 7077904 | tf_op jit(solution)/shard_map/all_gather | solution.py:21
  120.6 0.0 copy-done
  120.6 0.0 copy-done.2
  120.6 8.0 %fusion.9 = f32[448,1536]{1,0:T(8,128)} fusion(bf16[2304,1536]{1,0:T(8,128)(2,1)} %all-gather.4.cloned.1.call-done, bf16[448,2304]{1,0:T(8,128)(2,1)S(1)} %copy-done, f32[2304]{0:T(1024)S(1)} %copy-done.2, f32[448]{0:T(512)S(1)} %add_rsqrt_fusion.1), kind=kOutput, calls=%fused_computation.14 | convolution fusion | flops 3175022592 | bytes 11905792 | tf_op jit(solution)/shard_map/dot_general | solution.py:24
  128.5 100.7 %all-gather.6.cloned.1.call-done = bf16[2304,1536]{1,0:T(8,128)(2,1)} async-done(((bf16[288,1536]{1,0:T(8,128)(2,1)}), bf16[2304,1536]{1,0:T(8,128)(2,1)}) %all-gather.6.cloned.1.call-update) | async-done | bytes 7077904 | tf_op jit(solution)/shard_map/all_gather | solution.py:22
  229.3 108.7 %all-gather.8.cloned.1.call-done = bf16[1536,2304]{0,1:T(8,128)(2,1)} async-done(((bf16[1536,288]{0,1:T(8,128)(2,1)}), bf16[1536,2304]{0,1:T(8,128)(2,1)}) %all-gather.8.cloned.1.call-update) | async-done | bytes 7077904 | tf_op jit(solution)/shard_map/all_gather | solution.py:29
  338.0 13.9 %convolution_convert_fusion = bf16[448,2304]{1,0:T(8,128)(2,1)} fusion(bf16[1536,2304]{0,1:T(8,128)(2,1)} %all-gather.8.cloned.1.call-done, bf16[2304,1536]{1,0:T(8,128)(2,1)} %all-gather.6.cloned.1.call-done, f32[448,1536]{1,0:T(8,128)} %fusion.9, bf16[448,2304]{1,0:T(8,128)(2,1)S(1)} %copy-done, f32[2304]{0:T(1024)S(1)} %copy-done.2, ...), kind=kOutput, calls=%fused_computation.5 | convolution fusion | flops 6351077376 | bytes 21048064 | tf_op jit(solution)/shard_map/dot_general | solution.py:27
  351.9 0.0 copy-start.1
  351.9 0.0 all-reduce.2.cloned.1.call-update
  351.9 49.2 %all-reduce.2.cloned.1.call-done = bf16[448,2304]{1,0:T(8,128)(2,1)} async-done(((bf16[448,2304]{1,0:T(8,128)(2,1)}), bf16[448,2304]{1,0:T(8,128)(2,1)}) %all-reduce.2.cloned.1.call-update) | async-done | bytes 2064400 | tf_op jit(solution)/shard_map/psum | solution.py:32
  401.1 2.1 fusion
  403.2 0.0 copy-done.1
  403.2 3.8 fusion.5
  (2 shorter events, 0.0 us)
Async XLA Ops:
  6.5 114.0 %copy-start = (bf16[448,2304]{1,0:T(8,128)(2,1)S(1)}, bf16[448,2304]{1,0:T(8,128)(2,1)}, u32[]{:S(2)}) copy-start(bf16[448,2304]{1,0:T(8,128)(2,1)} %param.6) | copy-start | bytes 6193156
  6.5 114.0 %copy-start.2 = (f32[2304]{0:T(1024)S(1)}, f32[2304]{0:T(1024)}, u32[]{:S(2)}) copy-start(f32[2304]{0:T(1024)} %param.7) | copy-start | bytes 27652
  6.5 114.0 %all-gather.4.cloned.1.call-start = ((), (), s32[]{:S(2)}) async-start(), calls=%async_computation | async-start | bytes 7962624 | tf_op jit(solution)/shard_map/all_gather | solution.py:21
  7.3 222.0 %all-gather.6.cloned.1.call-start = ((), (), s32[]{:S(2)}) async-start(), calls=%async_computation.1 | async-start | bytes 7962624 | tf_op jit(solution)/shard_map/all_gather | solution.py:22
  8.0 330.0 %all-gather.8.cloned.1.call-start = ((), (), s32[]{:S(2)}) async-start(), calls=%async_computation.2 | async-start | bytes 7962624 | tf_op jit(solution)/shard_map/all_gather | solution.py:29
  8.7 392.4 %all-reduce.2.cloned.1.call-start = ((), (), s32[]{:S(2)}) async-start(), calls=%async_computation.3 | async-start | bytes 4128768 | tf_op jit(solution)/shard_map/psum | solution.py:32
  351.9 51.3 %copy-start.1 = (f32[2304]{0:T(1024)S(1)}, f32[2304]{0:T(1024)}, u32[]{:S(2)}) copy-start(f32[2304]{0:T(1024)} %param.11) | copy-start | bytes 27652
Sparse Core Ops, SparseCore 0:
  9.5 110.9 all-gather.3
  122.8 106.4 all-gather.5
  231.5 106.4 all-gather.7
  352.0 49.0 all-reduce.1
where the time goes:
time: 414 us; the launch traced here: 413 us
  waiting for transfers between devices  370 us (89%)
  matrix products  21.9 us (5%)
  between operations  13.1 us (3%)
  other arithmetic  7.92 us (2%)
    all_gather x1, waiting for transfers between devices, per_device(): lax.all_gather(gate_weight, 'fs', axis=0, tiled=True)  110 us
    all_gather x1, waiting for transfers between devices, per_device(): lax.all_gather(down_weight, 'fs', axis=1, tiled=True)  109 us
    all_gather x1, waiting for transfers between devices, per_device(): lax.all_gather(up_weight, 'fs', axis=0, tiled=True)  101 us
    psum x1, waiting for transfers between devices, per_device(): lax.psum(partial_value.astype(jnp.bfloat16), 'tp').astype(jnp.float32)  49.2 us
    dot_general x1, matrix products, per_device(): jnp.dot(hidden, lax.all_gather(down_weight, 'fs', axis=1, tiled=True), pr...  13.9 us
  transfers between devices with their start and end apart: 4, of which 4 were waited for; matrix products, arithmetic and copies ran while one was open for 2% of the time, Pallas kernels for 0%

commit v1 on v0

--- a/solution.py
+++ b/solution.py
@@ -1,9 +1,15 @@
+import functools
+
 import jax
 import jax.numpy as jnp
 from jax import lax
+from jax.experimental import pallas as pl
+from jax.experimental.pallas import tpu as pltpu
 from jax.sharding import PartitionSpec as P
 
+MESH = pl.DeviceIdType.MESH
 epsilon = 1e-06
+SUB = 3
 
 
 def complete(own_tokens, summed, branch_gain):
@@ -13,10 +19,14 @@
     )
 
 
-def per_device(tokens, norm_gain, gate_weight, up_weight, down_weight, branch_gain):
+def normalize(tokens, norm_gain):
     widened = tokens.astype(jnp.float32)
     scale = lax.rsqrt(jnp.mean(widened * widened, axis=-1, keepdims=True) + epsilon)
-    normed = (widened * scale * norm_gain).astype(jnp.bfloat16)
+    return (widened * scale * norm_gain).astype(jnp.bfloat16)
+
+
+def plain(tokens, norm_gain, gate_weight, up_weight, down_weight, branch_gain):
+    normed = normalize(tokens, norm_gain)
     gate_whole, up_whole = (
         lax.all_gather(gate_weight, "fs", axis=0, tiled=True),
         lax.all_gather(up_weight, "fs", axis=0, tiled=True),
@@ -33,9 +43,250 @@
     return complete(tokens, summed, branch_gain)
 
 
+def log2(n):
+    return n.bit_length() - 1
+
+
+def kernel(n_fs, n_tp, group, tokens_ref, normed_ref, gate_ref, up_ref, down_ref, gain_ref, out_ref, *scratch):
+    n_group = n_fs // group
+    stages = log2(group * n_tp)
+    tp_bits = log2(n_tp)
+    xs, wg, wu, wd, hid, own, fin = scratch[:7]
+    held = scratch[7:7 + stages]
+    arrived = scratch[7 + stages:7 + 2 * stages]
+    (loc_sem, w_send, w_recv, x_send, x_recv, y_send, y_recv, r_send, r_recv, o_send, o_recv) = scratch[7 + 2 * stages:]
+    f, t = lax.axis_index("fs"), lax.axis_index("tp")
+    g, q = f // group, f % group
+    rank = q * n_tp + t
+    depth, width = gate_ref.shape[0], wg.shape[1]
+    chunks, rq, cw = fin.shape
+    rows = n_tp * rq
+
+    barrier = pltpu.get_barrier_semaphore()
+    for k in range(1, n_fs):
+        pl.semaphore_signal(barrier, inc=1, device_id=((f + k) % n_fs, t), device_id_type=MESH)
+    for k in range(1, n_tp):
+        pl.semaphore_signal(barrier, inc=1, device_id=(f, (t + k) % n_tp), device_id_type=MESH)
+
+    at = pl.ds(pl.multiple_of(f * depth, depth), depth)
+    mine = pl.ds(pl.multiple_of(q * width, width), width)
+    local = [
+        pltpu.make_async_copy(normed_ref, xs.at[q], loc_sem.at[0]),
+        pltpu.make_async_copy(gate_ref.at[:, mine], wg.at[at], loc_sem.at[1]),
+        pltpu.make_async_copy(up_ref.at[:, mine], wu.at[at], loc_sem.at[2]),
+        pltpu.make_async_copy(down_ref.at[:, mine], wd.at[at], loc_sem.at[3]),
+        pltpu.make_async_copy(tokens_ref.at[t], own, loc_sem.at[4]),
+    ]
+    for copy in local:
+        copy.start()
+    pl.semaphore_wait(barrier, n_fs + n_tp - 2)
+
+    first = {}
+    for k in range(1, group):
+        first[k] = pltpu.make_async_remote_copy(
+            normed_ref.at[t], xs.at[q, t], x_send.at[k], x_recv.at[k],
+            device_id=(g * group + (q + k) % group, t), device_id_type=MESH,
+        )
+        first[k].start()
+    moved = {}
+    for a, (src, dst) in enumerate(((gate_ref, wg), (up_ref, wu), (down_ref, wd))):
+        for dg in reversed(range(n_group)):
+            for dq in range(group):
+                if dg + dq > 0:
+                    to_q = (q + dq) % group
+                    part = pl.ds(pl.multiple_of(to_q * width, width), width)
+                    moved[a, dg, dq] = pltpu.make_async_remote_copy(
+                        src.at[:, part], dst.at[at],
+                        w_send.at[a, dg * group + dq], w_recv.at[a, dg * group + dq],
+                        device_id=(((g + dg) % n_group) * group + to_q, t), device_id_type=MESH,
+                    )
+                    moved[a, dg, dq].start()
+    second = {}
+    for k in range(1, group):
+        first[k].wait_recv()
+        of = (q + group - k) % group
+        for m in range(1, n_tp):
+            second[k, m] = pltpu.make_async_remote_copy(
+                xs.at[of, t], xs.at[of, t], y_send.at[k, m], y_recv.at[k, m],
+                device_id=(f, (t + m) % n_tp), device_id_type=MESH,
+            )
+            second[k, m].start()
+    for copy in local:
+        copy.wait()
+    for copy in second.values():
+        copy.wait_recv()
+    for (a, dg, dq), copy in moved.items():
+        if a < 2:
+            copy.wait_recv()
+
+    def hidden_block(b, carry):
+        x = xs[b].reshape(rows, xs.shape[-1])
+        gate = jnp.dot(x, wg[...], preferred_element_type=jnp.float32)
+        up = jnp.dot(x, wu[...], preferred_element_type=jnp.float32)
+        hid[b] = (gate / (1.0 + jnp.exp(-gate)) * up).astype(jnp.bfloat16)
+        return carry
+
+    lax.fori_loop(0, group, hidden_block, 0)
+
+    def column(i):
+        return ((g + i // SUB) % n_group) * SUB + i % SUB
+
+    def reduction(i, s):
+        bit = (rank // 2**s) % 2
+        flip = 1 - 2 * bit
+        if s < tp_bits:
+            to = (f, t + flip * 2**s)
+        else:
+            to = (f + flip * 2 ** (s - tp_bits), t)
+        return pltpu.make_async_remote_copy(
+            held[s].at[i, :, 1 - bit], arrived[s].at[i], r_send.at[i, s], r_recv.at[i, s],
+            device_id=to, device_id_type=MESH,
+        )
+
+    def down_chunk(i):
+        if i % SUB == 0:
+            dg = (n_group - i // SUB) % n_group
+            for dq in range(group):
+                if dg + dq > 0:
+                    moved[2, dg, dq].wait_recv()
+        cols = pl.ds(pl.multiple_of(column(i) * cw, cw), cw)
+
+        def block(b, carry):
+            part = lax.dot_general(
+                hid[b], wd[cols, :], (((1,), (1,)), ((), ())), preferred_element_type=jnp.float32
+            ).astype(jnp.bfloat16)
+            held[0][i, pl.ds(b * (n_tp // 2), n_tp // 2)] = part.reshape(n_tp // 2, 2, rq, cw)
+            return carry
+
+        lax.fori_loop(0, group, block, 0)
+
+    def add_stage(i, s):
+        reduction(i, s).wait_recv()
+        bit = (rank // 2**s) % 2
+        if s == stages - 1:
+            fin[i] = held[s][i, 0, bit].astype(jnp.float32) + arrived[s][i, 0].astype(jnp.float32)
+            return
+
+        def one(j, carry):
+            total = held[s][i, j, bit].astype(jnp.float32) + arrived[s][i, j].astype(jnp.float32)
+            held[s + 1][i, j // 2, j % 2] = total.astype(jnp.bfloat16)
+            return carry
+
+        lax.fori_loop(0, held[s].shape[1], one, 0)
+
+    for step in range(chunks + stages):
+        for s in reversed(range(stages)):
+            i = step - s - 1
+            if 0 <= i < chunks:
+                add_stage(i, s)
+                if s + 1 < stages:
+                    reduction(i, s + 1).start()
+        if step < chunks:
+            down_chunk(step)
+            reduction(step, 0).start()
+
+    square = jnp.zeros((rq, 1), jnp.float32)
+    for i in range(chunks):
+        square += jnp.sum(fin[i] * fin[i], axis=-1, keepdims=True)
+    scale = lax.rsqrt(square * (1.0 / (chunks * cw)) + epsilon)
+    for i in range(chunks):
+        cols = pl.ds(pl.multiple_of(column(i) * cw, cw), cw)
+        out_ref[0, t, :, cols] = (
+            own[:, cols].astype(jnp.float32) + fin[i] * scale * gain_ref[:, cols]
+        ).astype(jnp.bfloat16)
+
+    shared = []
+    for s in reversed(range(tp_bits)):
+        bit = (t // 2**s) % 2
+        to = (f, t + (1 - 2 * bit) * 2**s)
+        known = range(2 ** (tp_bits - 1 - s))
+        batch = []
+        for h in known:
+            piece = out_ref.at[0, h * 2 ** (s + 1) + t % 2 ** (s + 1)]
+            batch.append(pltpu.make_async_remote_copy(
+                piece, piece, o_send.at[s, h], o_recv.at[s, h], device_id=to, device_id_type=MESH,
+            ))
+        for copy in batch:
+            copy.start()
+        for copy in batch:
+            copy.wait_recv()
+        shared += batch
+    for copy in list(first.values()) + list(moved.values()) + list(second.values()) + shared:
+        copy.wait_send()
+    for i in range(chunks):
+        for s in range(stages):
+            reduction(i, s).wait_send()
+
+
+def fused(n_fs, n_tp, group, tokens, norm_gain, gate_weight, up_weight, down_weight, branch_gain):
+    rows, d = tokens.shape
+    rq = rows // n_tp
+    depth, hidden = gate_weight.shape
+    width = hidden // group
+    chunks = (n_fs // group) * SUB
+    cw = d // chunks
+    pieces = group * n_tp
+    stages = log2(pieces)
+    normed = normalize(tokens, norm_gain)
+    bf16, dma = jnp.bfloat16, pltpu.SemaphoreType.DMA
+    hbm = pl.BlockSpec(memory_space=pl.ANY)
+    vmem = pl.BlockSpec(memory_space=pltpu.VMEM)
+    out = pl.pallas_call(
+        functools.partial(kernel, n_fs, n_tp, group),
+        out_shape=jax.ShapeDtypeStruct((1, n_tp, rq, d), bf16),
+        in_specs=[hbm] * 5 + [vmem],
+        out_specs=vmem,
+        scratch_shapes=[
+            pltpu.VMEM((group, n_tp, rq, d), bf16),
+            pltpu.VMEM((d, width), bf16),
+            pltpu.VMEM((d, width), bf16),
+            pltpu.VMEM((d, width), bf16),
+            pltpu.VMEM((group, rows, width), bf16),
+            pltpu.VMEM((rq, d), bf16),
+            pltpu.VMEM((chunks, rq, cw), jnp.float32),
+        ]
+        + [pltpu.VMEM((chunks, pieces >> (s + 1), 2, rq, cw), bf16) for s in range(stages)]
+        + [pltpu.VMEM((chunks, pieces >> (s + 1), rq, cw), bf16) for s in range(stages)]
+        + [
+            dma((5,)),
+            dma((3, n_fs)), dma((3, n_fs)),
+            dma((group,)), dma((group,)),
+            dma((group, n_tp)), dma((group, n_tp)),
+            dma((chunks, stages)), dma((chunks, stages)),
+            dma((log2(n_tp), n_tp)), dma((log2(n_tp), n_tp)),
+        ],
+        compiler_params=pltpu.CompilerParams(
+            collective_id=0, has_side_effects=True, vmem_limit_bytes=60 * 1024 * 1024
+        ),
+    )(
+        tokens.reshape(n_tp, rq, d), normed.reshape(n_tp, rq, d),
+        gate_weight, up_weight, down_weight.T, branch_gain.reshape(1, d),
+    )
+    return out.reshape(rows, d)
+
+
 def solution(mesh):
+    n_fs, n_tp = mesh.shape["fs"], mesh.shape["tp"]
+
+    def per_device(*args):
+        tokens, _, gate_weight = args[:3]
+        rows, d = tokens.shape
+        depth, hidden = gate_weight.shape
+        group = 4
+        fits = (
+            n_fs % group == 0
+            and n_tp & (n_tp - 1) == 0
+            and n_tp > 1
+            and rows % (16 * n_tp) == 0
+            and depth % 16 == 0
+            and hidden % (128 * group) == 0
+            and d % (128 * SUB * max(n_fs // group, 1)) == 0
+        )
+        if fits:
+            return fused(n_fs, n_tp, group, *args)
+        return plain(*args)
+
     in_specs = (P("fs", None), P(), P("fs", "tp"), P("fs", "tp"), P("tp", "fs"), P())
-    out_specs = P("fs", None)
     return jax.shard_map(
-        per_device, mesh=mesh, in_specs=in_specs, out_specs=out_specs, check_vma=False
-    )
+        per_device, mesh=mesh, in_specs=in_specs, out_specs=P("fs", None), check_vma=False
+    )

time: 414 us -> 215 us (0.52)
  waiting for transfers between devices: 370 us -> 0 us
  Pallas kernels: 0 us -> 206 us
  matrix products: 21.9 us -> 0 us
  between operations: 13.1 us -> 0.01 us
  local copies, waits for them, and re-layouts: 0.01 us -> 4.34 us
    all_gather x3 -> x0, waiting for transfers between devices: 319 us -> none  [the longest x1 110 us: per_device(): lax.all_gather(gate_weight, 'fs', axis=0, tiled=True)]
    pallas_call x0 -> x1, Pallas kernels: none -> 206 us  [fused(): pl.pallas_call(functools.partial(kernel, n_fs, n_tp, group), out_shape=ja...]
    psum x1 -> x0, waiting for transfers between devices: 49.2 us -> none  [per_device(): lax.psum(partial_value.astype(jnp.bfloat16), 'tp').astype(jnp.float32)]
    dot_general x2 -> x0, matrix products: 21.9 us -> none  [the longest x1 13.9 us: per_device(): jnp.dot(hidden, lax.all_gather(down_weight, 'fs', axis=1, tiled=True), pr...]
  transfers between devices with their start and end apart: 4 -> 0, of which waited for: 4 -> 0; matrix products, arithmetic and copies ran while one was open for 2% -> 0% of each run, Pallas kernels for 0% -> 0%
where the time goes in v1:
time: 215 us; the launch traced here: 214 us
  Pallas kernels  206 us (96%)
  local copies, waits for them, and re-layouts  4.34 us (2%)
  other arithmetic  4.06 us (2%)
    pallas_call x1, Pallas kernels, fused(): pl.pallas_call(functools.partial(kernel, n_fs, n_tp, group), out_shape=ja...  206 us

profile of v1, /device:TPU:0, one launch (start us, length us, event | category | flops | bytes accessed | tf_op | source)
XLA Modules:
  0.0 214.3 jit_solution(3968617876654605560)
XLA Ops:
  0.0 0.0 copy-start
  0.0 0.0 copy-start.1
  0.0 2.2 %fusion = f32[448]{0:T(512)S(1)} fusion(bf16[448,2304]{1,0:T(8,128)(2,1)} %param.6), kind=kLoop, calls=%fused_computation.2 | loop fusion | flops 3096128 | bytes 2066176 | tf_op jit(solution)/shard_map/reduce_sum | solution.py:24
  2.2 1.3 reshape.23.gain_ref
  3.5 0.0 copy-done
  3.5 0.0 copy-done.1
  3.5 1.8 fusion.2
  5.4 205.9 %shard_map.64 = bf16[1,4,112,2304]{3,2,1,0:T(8,128)(2,1)} custom-call(bf16[4,112,2304]{2,1,0:T(8,128)(2,1)} %bitcast.4, bf16[4,112,2304]{2,1,0:T(8,128)(2,1)} %bitcast.5, bf16[288,1536]{1,0:T(8,128)(2,1)} %gate_ref.1, bf16[288,1536]{1,0:T(8,128)(2,1)} %up_ref.1, bf16[288,1536]{1,0:T(8,128)(2,1)} %bitcast.7, f32[1,2304]{1,0:T(1,128)} %reshape.23.gain_ref), custom_call_target="tpu_custom_call" | custom-call | tf_op jit(solution)/shard_map/pallas_call | solution.py:234
  211.3 3.0 %copy.8 = bf16[448,2304]{1,0:T(8,128)(2,1)} copy(bf16[448,2304]{1,0:T(8,128)(2,1)} %bitcast.6) | data formatting | bytes 4128768
  (1 shorter events, 0.0 us)
Async XLA Ops:
  0.0 3.5 %copy-start = (bf16[448,2304]{1,0:T(8,128)(2,1)S(1)}, bf16[448,2304]{1,0:T(8,128)(2,1)}, u32[]{:S(2)}) copy-start(bf16[448,2304]{1,0:T(8,128)(2,1)} %param.6) | copy-start | bytes 6193156
  0.0 3.5 %copy-start.1 = (f32[2304]{0:T(1024)S(1)}, f32[2304]{0:T(1024)}, u32[]{:S(2)}) copy-start(f32[2304]{0:T(1024)} %param.7) | copy-start | bytes 27652

commit v2 on v1

v2 whole, which is shorter than its diff:
```python
import functools

import jax
import jax.numpy as jnp
from jax import lax
from jax.experimental import pallas as pl
from jax.experimental.pallas import tpu as pltpu
from jax.sharding import PartitionSpec as P

MESH = pl.DeviceIdType.MESH
epsilon = 1e-06
SUB = 3


def complete(own_tokens, summed, branch_gain):
    branch_scale = lax.rsqrt(jnp.mean(summed * summed, axis=-1, keepdims=True) + epsilon)
    return (own_tokens.astype(jnp.float32) + summed * branch_scale * branch_gain).astype(
        jnp.bfloat16
    )


def normalize(tokens, norm_gain):
    widened = tokens.astype(jnp.float32)
    scale = lax.rsqrt(jnp.mean(widened * widened, axis=-1, keepdims=True) + epsilon)
    return (widened * scale * norm_gain).astype(jnp.bfloat16)


def plain(tokens, norm_gain, gate_weight, up_weight, down_weight, branch_gain):
    normed = normalize(tokens, norm_gain)
    gate_whole, up_whole = (
        lax.all_gather(gate_weight, "fs", axis=0, tiled=True),
        lax.all_gather(up_weight, "fs", axis=0, tiled=True),
    )
    gate_sum = jnp.dot(normed, gate_whole, preferred_element_type=jnp.float32)
    up_sum = jnp.dot(normed, up_whole, preferred_element_type=jnp.float32)
    hidden = (jax.nn.silu(gate_sum) * up_sum).astype(jnp.bfloat16)
    partial_value = jnp.dot(
        hidden,
        lax.all_gather(down_weight, "fs", axis=1, tiled=True),
        preferred_element_type=jnp.float32,
    )
    summed = lax.psum(partial_value.astype(jnp.bfloat16), "tp").astype(jnp.float32)
    return complete(tokens, summed, branch_gain)


def log2(n):
    return n.bit_length() - 1


def kernel(n_fs, n_tp, group, tokens_ref, gate_ref, up_ref, down_ref, gain_ref, out_ref, *scratch):
    n_group = n_fs // group
    stages = log2(group * n_tp)
    tp_bits = log2(n_tp)
    xs, xn, wg, wu, wd, hid = scratch[:6]
    held = scratch[6:6 + stages]
    arrived = scratch[6 + stages:6 + 2 * stages]
    (loc_sem, w_send, w_recv, x_send, x_recv, y_send, y_recv, r_send, r_recv, o_send, o_recv) = scratch[6 + 2 * stages:]
    f, t = lax.axis_index("fs"), lax.axis_index("tp")
    g, q = f // group, f % group
    rank = q * n_tp + t
    depth, width = gate_ref.shape[0], wg.shape[1]
    chunks, rq, cw = arrived[0].shape[0], *arrived[0].shape[2:]
    rows = n_tp * rq

    barrier = pltpu.get_barrier_semaphore()
    for k in range(1, n_fs):
        pl.semaphore_signal(barrier, inc=1, device_id=((f + k) % n_fs, t), device_id_type=MESH)
    for k in range(1, n_tp):
        pl.semaphore_signal(barrier, inc=1, device_id=(f, (t + k) % n_tp), device_id_type=MESH)

    at = pl.ds(pl.multiple_of(f * depth, depth), depth)
    mine = pl.ds(pl.multiple_of(q * width, width), width)
    local = [
        pltpu.make_async_copy(tokens_ref, xs.at[q], loc_sem.at[0]),
        pltpu.make_async_copy(gate_ref.at[:, mine], wg.at[at], loc_sem.at[1]),
        pltpu.make_async_copy(up_ref.at[:, mine], wu.at[at], loc_sem.at[2]),
        pltpu.make_async_copy(down_ref.at[:, mine], wd.at[at], loc_sem.at[3]),
    ]
    for copy in local:
        copy.start()
    pl.semaphore_wait(barrier, n_fs + n_tp - 2)

    first = {}
    for k in range(1, group):
        first[k] = pltpu.make_async_remote_copy(
            tokens_ref.at[t], xs.at[q, t], x_send.at[k], x_recv.at[k],
            device_id=(g * group + (q + k) % group, t), device_id_type=MESH,
        )
        first[k].start()
    moved = {}
    for a, (src, dst) in enumerate(((gate_ref, wg), (up_ref, wu), (down_ref, wd))):
        for dg in reversed(range(n_group)) if a < 2 else range(n_group):
            for dq in range(group):
                if dg + dq > 0:
                    to_q = (q + dq) % group
                    part = pl.ds(pl.multiple_of(to_q * width, width), width)
                    moved[a, dg, dq] = pltpu.make_async_remote_copy(
                        src.at[:, part], dst.at[at],
                        w_send.at[a, dg * group + dq], w_recv.at[a, dg * group + dq],
                        device_id=(((g + dg) % n_group) * group + to_q, t), device_id_type=MESH,
                    )
                    moved[a, dg, dq].start()
    def normalize_piece(block, piece):
        def strip(r, carry):
            at_rows = pl.ds(pl.multiple_of(r * 16, 16), 16)
            x = xs[block, piece, at_rows, :].astype(jnp.float32)
            scale = lax.rsqrt(jnp.mean(x * x, axis=-1, keepdims=True) + epsilon)
            xn[block, piece, at_rows, :] = (x * scale * gain_ref[...]).astype(jnp.bfloat16)
            return carry

        lax.fori_loop(0, rq // 16, strip, 0)

    for copy in local:
        copy.wait()
    for piece in range(n_tp):
        normalize_piece(q, piece)
    second = {}
    for k in range(1, group):
        first[k].wait_recv()
        of = (q + group - k) % group
        for m in range(1, n_tp):
            second[k, m] = pltpu.make_async_remote_copy(
                xs.at[of, t], xs.at[of, t], y_send.at[k, m], y_recv.at[k, m],
                device_id=(f, (t + m) % n_tp), device_id_type=MESH,
            )
            second[k, m].start()
        normalize_piece(of, t)
    for (k, m), copy in second.items():
        copy.wait_recv()
        normalize_piece((q + group - k) % group, (t + n_tp - m) % n_tp)
    for (a, dg, dq), copy in moved.items():
        if a < 2:
            copy.wait_recv()

    def hidden_block(b, carry):
        x = xn[b].reshape(rows, xn.shape[-1])
        gate = jnp.dot(x, wg[...], preferred_element_type=jnp.float32)
        up = jnp.dot(x, wu[...], preferred_element_type=jnp.float32)
        hid[b] = (gate / (1.0 + jnp.exp(-gate)) * up).astype(jnp.bfloat16)
        return carry

    lax.fori_loop(0, group, hidden_block, 0)

    def column(i):
        return ((g + i // SUB) % n_group) * SUB + i % SUB

    def order(i):
        rest = list(range(1, stages))
        turn = i % SUB % len(rest)
        return [0] + rest[turn:] + rest[:turn]

    def reduction(i, s):
        b = order(i)[s]
        bit = (rank // 2**b) % 2
        flip = 1 - 2 * bit
        if b < tp_bits:
            to = (f, t + flip * 2**b)
        else:
            to = (f + flip * 2 ** (b - tp_bits), t)
        return pltpu.make_async_remote_copy(
            held[s].at[i, :, 1 - bit], arrived[s].at[i], r_send.at[i, s], r_recv.at[i, s],
            device_id=to, device_id_type=MESH,
        )

    def columns(i):
        return pl.ds(pl.multiple_of(column(i) * cw, cw), cw)

    def down_chunk(i):
        def block(b, carry):
            part = lax.dot_general(
                hid[b], wd[columns(i), :], (((1,), (1,)), ((), ())),
                preferred_element_type=jnp.float32,
            ).astype(jnp.bfloat16)
            for piece in range(n_tp):
                owner = b * n_tp + piece
                place = sum((owner // 2**o) % 2 * 2**s for s, o in enumerate(order(i)))
                held[0][i, place // 2, place % 2] = part[piece * rq:(piece + 1) * rq]
            return carry

        lax.fori_loop(0, group, block, 0)

    def add_stage(i, s):
        reduction(i, s).wait_recv()
        bit = (rank // 2 ** order(i)[s]) % 2
        if s == stages - 1:
            total = held[s][i, 0, bit].astype(jnp.float32) + arrived[s][i, 0].astype(jnp.float32)
            out_ref[0, t, :, columns(i)] = total.astype(jnp.bfloat16)
            return

        def one(j, carry):
            total = held[s][i, j, bit].astype(jnp.float32) + arrived[s][i, j].astype(jnp.float32)
            held[s + 1][i, j // 2, j % 2] = total.astype(jnp.bfloat16)
            return carry

        lax.fori_loop(0, held[s].shape[1], one, 0)

    def sharing(i, s):
        bit = (t // 2**s) % 2
        copies = []
        for h in range(2 ** (tp_bits - 1 - s)):
            piece = out_ref.at[0, h * 2 ** (s + 1) + t % 2 ** (s + 1), :, columns(i)]
            copies.append(pltpu.make_async_remote_copy(
                piece, piece, o_send.at[i, s, h], o_recv.at[i, s, h],
                device_id=(f, t + (1 - 2 * bit) * 2**s), device_id_type=MESH,
            ))
        return copies

    for part in range(n_group):
        dg = (n_group - part) % n_group
        for dq in range(group):
            if dg + dq > 0:
                moved[2, dg, dq].wait_recv()
        here = range(part * SUB, (part + 1) * SUB)
        for i in here:
            down_chunk(i)
            reduction(i, 0).start()
        for s in range(stages):
            for i in here:
                add_stage(i, s)
                if s + 1 < stages:
                    reduction(i, s + 1).start()
                else:
                    for copy in sharing(i, tp_bits - 1):
                        copy.start()
        for s in reversed(range(tp_bits)):
            for i in here:
                for copy in sharing(i, s):
                    copy.wait_recv()
                if s > 0:
                    for copy in sharing(i, s - 1):
                        copy.start()

    for copy in list(first.values()) + list(moved.values()) + list(second.values()):
        copy.wait_send()
    for i in range(chunks):
        for s in range(stages):
            reduction(i, s).wait_send()
        for s in range(tp_bits):
            for copy in sharing(i, s):
                copy.wait_send()


def fused(n_fs, n_tp, group, tokens, norm_gain, gate_weight, up_weight, down_weight, branch_gain):
    rows, d = tokens.shape
    rq = rows // n_tp
    depth, hidden = gate_weight.shape
    width = hidden // group
    chunks = (n_fs // group) * SUB
    cw = d // chunks
    pieces = group * n_tp
    stages = log2(pieces)
    bf16, dma = jnp.bfloat16, pltpu.SemaphoreType.DMA
    hbm = pl.BlockSpec(memory_space=pl.ANY)
    vmem = pl.BlockSpec(memory_space=pltpu.VMEM)
    out = pl.pallas_call(
        functools.partial(kernel, n_fs, n_tp, group),
        out_shape=jax.ShapeDtypeStruct((1, n_tp, rq, d), bf16),
        in_specs=[hbm] * 4 + [vmem],
        out_specs=vmem,
        scratch_shapes=[
            pltpu.VMEM((group, n_tp, rq, d), bf16),
            pltpu.VMEM((group, n_tp, rq, d), bf16),
            pltpu.VMEM((d, width), bf16),
            pltpu.VMEM((d, width), bf16),
            pltpu.VMEM((d, width), bf16),
            pltpu.VMEM((group, rows, width), bf16),
        ]
        + [pltpu.VMEM((chunks, pieces >> (s + 1), 2, rq, cw), bf16) for s in range(stages)]
        + [pltpu.VMEM((chunks, pieces >> (s + 1), rq, cw), bf16) for s in range(stages)]
        + [
            dma((4,)),
            dma((3, n_fs)), dma((3, n_fs)),
            dma((group,)), dma((group,)),
            dma((group, n_tp)), dma((group, n_tp)),
            dma((chunks, stages)), dma((chunks, stages)),
            dma((chunks, log2(n_tp), n_tp)), dma((chunks, log2(n_tp), n_tp)),
        ],
        compiler_params=pltpu.CompilerParams(
            collective_id=0, has_side_effects=True, vmem_limit_bytes=60 * 1024 * 1024
        ),
    )(
        tokens.reshape(n_tp, rq, d), gate_weight, up_weight, down_weight.T, norm_gain.reshape(1, d),
    )
    return complete(tokens, out.reshape(rows, d).astype(jnp.float32), branch_gain)


def solution(mesh):
    n_fs, n_tp = mesh.shape["fs"], mesh.shape["tp"]

    def per_device(*args):
        tokens, _, gate_weight = args[:3]
        rows, d = tokens.shape
        depth, hidden = gate_weight.shape
        group = 4
        fits = (
            n_fs % group == 0
            and n_tp & (n_tp - 1) == 0
            and n_tp > 1
            and rows % (16 * n_tp) == 0
            and depth % 16 == 0
            and hidden % (128 * group) == 0
            and d % (128 * SUB * max(n_fs // group, 1)) == 0
        )
        if fits:
            return fused(n_fs, n_tp, group, *args)
        return plain(*args)

    in_specs = (P("fs", None), P(), P("fs", "tp"), P("fs", "tp"), P("tp", "fs"), P())
    return jax.shard_map(
        per_device, mesh=mesh, in_specs=in_specs, out_specs=P("fs", None), check_vma=False
    )
```

time: 215 us -> 190 us (0.88)
  Pallas kernels: 206 us -> 183 us
  local copies, waits for them, and re-layouts: 4.34 us -> 1.41 us
    pallas_call x1, Pallas kernels: 206 us -> 183 us  [fused(): pl.pallas_call(functools.partial(kernel, n_fs, n_tp, group), out_shape=ja...]
    unnamed x5 -> x4, local copies, waits for them, and re-layouts: 3.02 us -> 0.01 us
where the time goes in v2:
time: 190 us
  Pallas kernels  183 us (96%)
  other arithmetic  6 us (3%)
    pallas_call x1, Pallas kernels, fused(): pl.pallas_call(functools.partial(kernel, n_fs, n_tp, group), out_shape=ja...  183 us

profile of v2, /device:TPU:0, one launch (start us, length us, event | category | flops | bytes accessed | tf_op | source)
XLA Modules:
  0.0 190.2 jit_solution(307955675085182477)
XLA Ops:
  0.0 1.3 reshape.28.gain_ref
  1.3 0.0 copy-start.1
  1.3 182.7 %shard_map.64 = bf16[1,4,112,2304]{3,2,1,0:T(8,128)(2,1)} custom-call(bf16[4,112,2304]{2,1,0:T(8,128)(2,1)} %bitcast.10, bf16[288,1536]{1,0:T(8,128)(2,1)} %gate_ref.1, bf16[288,1536]{1,0:T(8,128)(2,1)} %up_ref.1, bf16[288,1536]{1,0:T(8,128)(2,1)} %bitcast.11, f32[1,2304]{1,0:T(1,128)} %reshape.28.gain_ref), custom_call_target="tpu_custom_call" | custom-call | tf_op jit(solution)/shard_map/pallas_call | solution.py:255
  184.1 0.0 copy-start
  184.1 2.2 %multiply_reduce_fusion = f32[4,112]{1,0:T(4,128)S(1)} fusion(bf16[1,4,112,2304]{3,2,1,0:T(8,128)(2,1)} %shard_map.64), kind=kLoop, calls=%fused_computation.4 | loop fusion | flops 3096128 | bytes 2066176 | tf_op jit(solution)/shard_map/reduce_sum | solution.py:16
  186.3 0.1 rsqrt.12
  186.4 0.0 copy-done.1
  186.4 0.0 copy-done
  186.4 3.8 %fusion.2 = bf16[448,2304]{1,0:T(8,128)(2,1)} fusion(bf16[448,2304]{1,0:T(8,128)(2,1)} %param.6, f32[2304]{0:T(1024)S(1)} %copy-done.1, f32[448]{0:T(512)S(1)} %rsqrt.12, bf16[1,4,112,2304]{3,2,1,0:T(8,128)(2,1)S(1)} %copy-done), kind=kLoop, calls=%fused_computation.3 | loop fusion | flops 6193152 | bytes 6204160 | tf_op jit(solution)/shard_map/convert_element_type | solution.py:17
  (1 shorter events, 0.0 us)
Async XLA Ops:
  1.3 185.1 %copy-start.1 = (f32[2304]{0:T(1024)S(1)}, f32[2304]{0:T(1024)}, u32[]{:S(2)}) copy-start(f32[2304]{0:T(1024)} %param.11) | copy-start | bytes 27652
  184.1 2.3 %copy-start = (bf16[1,4,112,2304]{3,2,1,0:T(8,128)(2,1)S(1)}, bf16[1,4,112,2304]{3,2,1,0:T(8,128)(2,1)}, u32[]{:S(2)}) copy-start(bf16[1,4,112,2304]{3,2,1,0:T(8,128)(2,1)} %shard_map.64) | copy-start | bytes 6193156

commit v3 on v2

--- a/solution.py
+++ b/solution.py
@@ -10,6 +10,7 @@
 MESH = pl.DeviceIdType.MESH
 epsilon = 1e-06
 SUB = 3
+LAG = 2
 
 
 def complete(own_tokens, summed, branch_gain):
@@ -51,10 +52,10 @@
     n_group = n_fs // group
     stages = log2(group * n_tp)
     tp_bits = log2(n_tp)
-    xs, xn, wg, wu, wd, hid = scratch[:6]
-    held = scratch[6:6 + stages]
-    arrived = scratch[6 + stages:6 + 2 * stages]
-    (loc_sem, w_send, w_recv, x_send, x_recv, y_send, y_recv, r_send, r_recv, o_send, o_recv) = scratch[6 + 2 * stages:]
+    xs, xn, wg, wu, wd, hid, gated = scratch[:7]
+    held = scratch[7:7 + stages]
+    arrived = scratch[7 + stages:7 + 2 * stages]
+    (loc_sem, w_send, w_recv, x_send, x_recv, y_send, y_recv, r_send, r_recv, o_send, o_recv) = scratch[7 + 2 * stages:]
     f, t = lax.axis_index("fs"), lax.axis_index("tp")
     g, q = f // group, f % group
     rank = q * n_tp + t
@@ -114,32 +115,55 @@
         copy.wait()
     for piece in range(n_tp):
         normalize_piece(q, piece)
-    second = {}
+    def spread(k, s):
+        of = (q + group - k) % group
+        bit = (t // 2**s) % 2
+        copies = []
+        for h in range(2 ** (tp_bits - 1 - s)):
+            piece = xs.at[of, h * 2 ** (s + 1) + t % 2 ** (s + 1)]
+            copies.append(pltpu.make_async_remote_copy(
+                piece, piece, y_send.at[k, s, h], y_recv.at[k, s, h],
+                device_id=(f, t + (1 - 2 * bit) * 2**s), device_id_type=MESH,
+            ))
+        return copies
+
     for k in range(1, group):
         first[k].wait_recv()
-        of = (q + group - k) % group
-        for m in range(1, n_tp):
-            second[k, m] = pltpu.make_async_remote_copy(
-                xs.at[of, t], xs.at[of, t], y_send.at[k, m], y_recv.at[k, m],
-                device_id=(f, (t + m) % n_tp), device_id_type=MESH,
-            )
-            second[k, m].start()
-        normalize_piece(of, t)
-    for (k, m), copy in second.items():
-        copy.wait_recv()
-        normalize_piece((q + group - k) % group, (t + n_tp - m) % n_tp)
-    for (a, dg, dq), copy in moved.items():
-        if a < 2:
-            copy.wait_recv()
-
-    def hidden_block(b, carry):
+        for copy in spread(k, tp_bits - 1):
+            copy.start()
+        normalize_piece((q + group - k) % group, t)
+    for s in reversed(range(tp_bits)):
+        other = (t % 2 ** (s + 1) + 2**s) % 2 ** (s + 1)
+        for k in range(1, group):
+            for copy in spread(k, s):
+                copy.wait_recv()
+            if s > 0:
+                for copy in spread(k, s - 1):
+                    copy.start()
+            for h in range(2 ** (tp_bits - 1 - s)):
+                normalize_piece((q + group - k) % group, h * 2 ** (s + 1) + other)
+
+    def arrived_weight(a):
+        for (b, _, _), copy in moved.items():
+            if a == b:
+                copy.wait_recv()
+
+    def gate_block(b, carry):
         x = xn[b].reshape(rows, xn.shape[-1])
         gate = jnp.dot(x, wg[...], preferred_element_type=jnp.float32)
+        gated[b] = gate / (1.0 + jnp.exp(-gate))
+        return carry
+
+    def up_block(b, carry):
+        x = xn[b].reshape(rows, xn.shape[-1])
         up = jnp.dot(x, wu[...], preferred_element_type=jnp.float32)
-        hid[b] = (gate / (1.0 + jnp.exp(-gate)) * up).astype(jnp.bfloat16)
+        hid[b] = (gated[b] * up).astype(jnp.bfloat16)
         return carry
 
-    lax.fori_loop(0, group, hidden_block, 0)
+    arrived_weight(0)
+    lax.fori_loop(0, group, gate_block, 0)
+    arrived_weight(1)
+    lax.fori_loop(0, group, up_block, 0)
 
     def column(i):
         return ((g + i // SUB) % n_group) * SUB + i % SUB
@@ -205,33 +229,49 @@
             ))
         return copies
 
-    for part in range(n_group):
+    def begin(part):
         dg = (n_group - part) % n_group
         for dq in range(group):
             if dg + dq > 0:
                 moved[2, dg, dq].wait_recv()
-        here = range(part * SUB, (part + 1) * SUB)
-        for i in here:
+        for i in range(part * SUB, (part + 1) * SUB):
             down_chunk(i)
             reduction(i, 0).start()
-        for s in range(stages):
-            for i in here:
-                add_stage(i, s)
-                if s + 1 < stages:
-                    reduction(i, s + 1).start()
-                else:
-                    for copy in sharing(i, tp_bits - 1):
-                        copy.start()
-        for s in reversed(range(tp_bits)):
-            for i in here:
-                for copy in sharing(i, s):
-                    copy.wait_recv()
-                if s > 0:
-                    for copy in sharing(i, s - 1):
-                        copy.start()
-
-    for copy in list(first.values()) + list(moved.values()) + list(second.values()):
+
+    def advance(part, s):
+        for i in range(part * SUB, (part + 1) * SUB):
+            add_stage(i, s)
+            if s + 1 < stages:
+                reduction(i, s + 1).start()
+            else:
+                for copy in sharing(i, tp_bits - 1):
+                    copy.start()
+
+    def share(part, s):
+        for i in range(part * SUB, (part + 1) * SUB):
+            for copy in sharing(i, s):
+                copy.wait_recv()
+            if s > 0:
+                for copy in sharing(i, s - 1):
+                    copy.start()
+
+    total_steps = 1 + stages + tp_bits
+    for slot in range(total_steps + LAG * (n_group - 1)):
+        for part in reversed(range(n_group)):
+            step = slot - LAG * part
+            if step == 0:
+                begin(part)
+            elif 1 <= step <= stages:
+                advance(part, step - 1)
+            elif stages < step < total_steps:
+                share(part, tp_bits - 1 - (step - 1 - stages))
+
+    for copy in list(first.values()) + list(moved.values()):
         copy.wait_send()
+    for k in range(1, group):
+        for s in range(tp_bits):
+            for copy in spread(k, s):
+                copy.wait_send()
     for i in range(chunks):
         for s in range(stages):
             reduction(i, s).wait_send()
@@ -264,6 +304,7 @@
             pltpu.VMEM((d, width), bf16),
             pltpu.VMEM((d, width), bf16),
             pltpu.VMEM((group, rows, width), bf16),
+            pltpu.VMEM((group, rows, width), jnp.float32),
         ]
         + [pltpu.VMEM((chunks, pieces >> (s + 1), 2, rq, cw), bf16) for s in range(stages)]
         + [pltpu.VMEM((chunks, pieces >> (s + 1), rq, cw), bf16) for s in range(stages)]
@@ -271,7 +312,7 @@
             dma((4,)),
             dma((3, n_fs)), dma((3, n_fs)),
             dma((group,)), dma((group,)),
-            dma((group, n_tp)), dma((group, n_tp)),
+            dma((group, log2(n_tp), n_tp)), dma((group, log2(n_tp), n_tp)),
             dma((chunks, stages)), dma((chunks, stages)),
             dma((chunks, log2(n_tp), n_tp)), dma((chunks, log2(n_tp), n_tp)),
         ],

time: 190 us -> 179 us (0.942)
  Pallas kernels: 183 us -> 171 us
    pallas_call x1, Pallas kernels: 183 us -> 171 us  [fused(): pl.pallas_call(functools.partial(kernel, n_fs, n_tp, group), out_shape=ja...]
where the time goes in v3:
time: 179 us
  Pallas kernels  171 us (96%)
  other arithmetic  6 us (3%)
    pallas_call x1, Pallas kernels, fused(): pl.pallas_call(functools.partial(kernel, n_fs, n_tp, group), out_shape=ja...  171 us
    convert_element_type x1, other arithmetic, complete(): (own_tokens.astype(jnp.float32) + summed * branch_scale * branch_gain).as...  3.78 us

profile of v3, /device:TPU:0, one launch (start us, length us, event | category | flops | bytes accessed | tf_op | source)
XLA Modules:
  0.0 178.9 jit_solution(8898102910942326204)
XLA Ops:
  0.0 1.3 reshape.28.gain_ref
  1.3 0.0 copy-start.1
  1.3 171.4 %shard_map.64 = bf16[1,4,112,2304]{3,2,1,0:T(8,128)(2,1)} custom-call(bf16[4,112,2304]{2,1,0:T(8,128)(2,1)} %bitcast.10, bf16[288,1536]{1,0:T(8,128)(2,1)} %gate_ref.1, bf16[288,1536]{1,0:T(8,128)(2,1)} %up_ref.1, bf16[288,1536]{1,0:T(8,128)(2,1)} %bitcast.11, f32[1,2304]{1,0:T(1,128)} %reshape.28.gain_ref), custom_call_target="tpu_custom_call" | custom-call | tf_op jit(solution)/shard_map/pallas_call | solution.py:295
  172.7 0.0 copy-start
  172.8 2.2 %multiply_reduce_fusion = f32[4,112]{1,0:T(4,128)S(1)} fusion(bf16[1,4,112,2304]{3,2,1,0:T(8,128)(2,1)} %shard_map.64), kind=kLoop, calls=%fused_computation.4 | loop fusion | flops 3096128 | bytes 2066176 | tf_op jit(solution)/shard_map/reduce_sum | solution.py:17
  175.0 0.1 rsqrt.12
  175.1 0.0 copy-done.1
  175.1 0.0 copy-done
  175.1 3.8 %fusion.2 = bf16[448,2304]{1,0:T(8,128)(2,1)} fusion(bf16[448,2304]{1,0:T(8,128)(2,1)} %param.6, f32[2304]{0:T(1024)S(1)} %copy-done.1, f32[448]{0:T(512)S(1)} %rsqrt.12, bf16[1,4,112,2304]{3,2,1,0:T(8,128)(2,1)S(1)} %copy-done), kind=kLoop, calls=%fused_computation.3 | loop fusion | flops 6193152 | bytes 6204160 | tf_op jit(solution)/shard_map/convert_element_type | solution.py:18
  (1 shorter events, 0.0 us)
Async XLA Ops:
  1.3 173.8 %copy-start.1 = (f32[2304]{0:T(1024)S(1)}, f32[2304]{0:T(1024)}, u32[]{:S(2)}) copy-start(f32[2304]{0:T(1024)} %param.11) | copy-start | bytes 27652
  172.7 2.3 %copy-start = (bf16[1,4,112,2304]{3,2,1,0:T(8,128)(2,1)S(1)}, bf16[1,4,112,2304]{3,2,1,0:T(8,128)(2,1)}, u32[]{:S(2)}) copy-start(bf16[1,4,112,2304]{3,2,1,0:T(8,128)(2,1)} %shard_map.64) | copy-start | bytes 6193156
